TPU v7x, 32 devices: a whole 2x2x4 slice. The times are simulated.
32 devices in a mesh: dp: 4 (over y, x), kv: 4 (over z), tp: 2 (over core).
Axes of the slice: x: 2, y: 2, z: 4, core: 2. Of those that a mesh axis runs over, the one named last changes fastest.
Arguments:
- tokens: bfloat16 [4, 1024, 2048], P('dp', 'kv'), may hold values from -28 to 28, as said below
- query_weight: bfloat16 [2048, 768], P(None, 'tp'), may hold values from -0.125 to 0.125
- key_weight: bfloat16 [2048, 256], P(None, 'tp'), may hold values from -0.125 to 0.125
- value_weight: bfloat16 [2048, 256], P(None, 'tp'), may hold values from -0.125 to 0.125
- gate_weight: bfloat16 [2048, 24], replicated, may hold values from -0.125 to 0.125
- compress_weight: float32 [2, 32, 64], replicated, may hold values from -1 to 1
- out_weight: bfloat16 [768, 2048], P('tp'), may hold values from -0.21875 to 0.21875
- out_gain: float32 [2048], replicated, may hold values from 0.1 to 1.9
- chosen: int32 [4, 32, 16], P('dp', 'kv'), may hold values from -1 to 31, as said below
Outputs:
- output: float32 [4, 1024, 2048], P('dp', ('kv', 'tp'))
Inputs may be any that keep to these rules, and one draw needn't show every extreme that they name: `chosen`: row q of a sequence lists distinct blocks; its first entry is q itself; the others are -1 or blocks held by an earlier index of kv (block index // 8). Over the rows of one kv index, at most 2 distinct blocks come from any other single index, and every index past the first reads exactly 2 blocks of the first index, among them block 0. `tokens`: finite activations; some rows are much larger than others in some draws.
All inputs are finite; a program needn't handle non-finite values.
Results may differ from a plain program's by a relative error of at most 0.02.
The roundings to bfloat16 on the way count: a program that leaves them out, or rounds other values in their place, can miss the bound.
Values may be sent and summed in bfloat16 or wider, within the bound.
A program may use at most 64 MiB of HBM per device.

v0:
```python
import jax
import jax.numpy as jnp
from jax import lax
from jax.sharding import PartitionSpec as P

HEAD = 64
BLK = 32
CAP = 2


neg_big = -1e30
rope_base = 500000.0
norm_eps = 1e-06


def rotate(array_in, positions):
    half_dim = array_in.shape[-1] // 2
    inverse = rope_base ** (-jnp.arange(half_dim, dtype=jnp.float32) * (2.0 / array_in.shape[-1]))
    angles = positions.astype(jnp.float32)[:, None] * inverse[None, :]
    cosine = jnp.cos(angles)[:, None, :]
    sine_vals = jnp.sin(angles)[:, None, :]
    floats = array_in.astype(jnp.float32)
    first_half = floats[..., :half_dim]
    second_half = floats[..., half_dim:]
    turned = jnp.concatenate(
        [
            first_half * cosine - second_half * sine_vals,
            second_half * cosine + first_half * sine_vals,
        ],
        axis=-1,
    )
    return turned.astype(jnp.bfloat16)


def absorb(
    partial_value, queries, key_flat, value_flat, block_ids, key_pos, member_table, query_pos
):
    running_max, weight_sum, weighted = partial_value
    amount = key_flat.shape[0]
    kv_dev = queries.shape[1]
    key_part = key_flat.reshape(amount, kv_dev, -1)
    value_part = value_flat.reshape(amount, kv_dev, -1)
    listed = (
        jnp.any(member_table[:, :, None] == block_ids[None, None, :], axis=1)
        & (block_ids >= 0)[None, :]
    )
    length = queries.shape[0]
    per_row = jnp.broadcast_to(
        listed[:, None, :], (listed.shape[0], length // listed.shape[0], amount)
    ).reshape(length, amount)
    allowed = per_row & (key_pos[None, :] <= query_pos[:, None])
    scores = jnp.einsum(
        "qhgd,khd->qhgk", queries, key_part, preferred_element_type=jnp.float32
    ) * queries.shape[-1] ** (-0.5)
    keep_mask = allowed[:, None, None, :]
    scores = jnp.where(keep_mask, scores, neg_big)
    new_max = jnp.maximum(running_max, jnp.max(scores, axis=-1))
    powers = jnp.where(keep_mask, jnp.exp(scores - new_max[..., None]), 0.0)
    shrink = jnp.exp(running_max - new_max)
    weight_sum = weight_sum * shrink + jnp.sum(powers, axis=-1)
    weighted = weighted * shrink[..., None] + jnp.einsum(
        "qhgk,khd->qhgd",
        powers.astype(jnp.bfloat16),
        value_part,
        preferred_element_type=jnp.float32,
    )
    return (new_max, weight_sum, weighted)


def absorb_span(
    partial_value, queries, key_flat, value_flat, block_ids, key_pos, member_table, query_pos
):
    amount = key_flat.shape[0]
    span_rows = 512
    if amount <= span_rows or amount % span_rows != 0:
        return absorb(
            partial_value,
            queries,
            key_flat,
            value_flat,
            block_ids,
            key_pos,
            member_table,
            query_pos,
        )
    rounds = amount // span_rows

    def advance(carried, pieces):
        return (
            absorb(
                carried,
                queries,
                pieces[0],
                pieces[1],
                pieces[2],
                pieces[3],
                member_table,
                query_pos,
            ),
            None,
        )

    carried, unused = lax.scan(
        advance,
        partial_value,
        (
            key_flat.reshape(rounds, span_rows, -1),
            value_flat.reshape(rounds, span_rows, -1),
            block_ids.reshape(rounds, span_rows),
            key_pos.reshape(rounds, span_rows),
        ),
    )
    return carried


def on_device(
    tokens,
    query_weight,
    key_weight,
    value_weight,
    gate_weight,
    compress_weight,
    out_weight,
    out_gain,
    chosen,
):
    source = tokens[0]
    length = source.shape[0]
    kv_dev = key_weight.shape[1] // HEAD
    heads_dev = query_weight.shape[1] // HEAD
    per_kv = heads_dev // kv_dev
    columns = kv_dev * HEAD
    blocks = length // BLK
    offset = lax.axis_index("kv") * length
    query_pos = offset + jnp.arange(length, dtype=jnp.int32)
    queries = jnp.dot(source, query_weight, preferred_element_type=jnp.float32).astype(jnp.bfloat16)
    key_rows = jnp.dot(source, key_weight, preferred_element_type=jnp.float32).astype(jnp.bfloat16)
    values = jnp.dot(source, value_weight, preferred_element_type=jnp.float32).astype(jnp.bfloat16)
    logits = jnp.dot(source, gate_weight, preferred_element_type=jnp.float32)
    first_head = lax.axis_index("tp") * heads_dev
    gate_cmp = jax.nn.sigmoid(lax.dynamic_slice_in_dim(logits, first_head, heads_dev, 1)).reshape(
        length, kv_dev, per_kv
    )
    gate_slc = jax.nn.sigmoid(
        lax.dynamic_slice_in_dim(logits, logits.shape[1] // 2 + first_head, heads_dev, 1)
    ).reshape(length, kv_dev, per_kv)
    plain_query = queries.reshape(length, kv_dev, per_kv, HEAD)
    turned_query = rotate(queries.reshape(length, heads_dev, HEAD), query_pos).reshape(
        length, kv_dev, per_kv, HEAD
    )
    turned_keys = rotate(key_rows.reshape(length, kv_dev, HEAD), query_pos).reshape(length, columns)
    key_blocks = key_rows.reshape(blocks, BLK, kv_dev, HEAD).astype(jnp.float32)
    val_blocks = values.reshape(blocks, BLK, kv_dev, HEAD).astype(jnp.float32)
    packed_keys = (
        jnp.einsum("njhd,jd->nhd", key_blocks, compress_weight[0], precision=lax.Precision.HIGHEST)
        .astype(jnp.bfloat16)
        .reshape(blocks, columns)
    )
    packed_values = (
        jnp.einsum("njhd,jd->nhd", val_blocks, compress_weight[1], precision=lax.Precision.HIGHEST)
        .astype(jnp.bfloat16)
        .reshape(blocks, columns)
    )
    summary_keys, summary_values = (
        lax.all_gather(packed_keys, "kv", axis=0, tiled=True),
        lax.all_gather(packed_values, "kv", axis=0, tiled=True),
    )
    summary = summary_keys.shape[0]
    scores = jnp.einsum(
        "qhgd,nhd->qhgn",
        plain_query,
        summary_keys.reshape(summary, kv_dev, HEAD),
        preferred_element_type=jnp.float32,
    ) * HEAD ** (-0.5)
    visible = ((jnp.arange(summary, dtype=jnp.int32) + 1) * BLK - 1)[None, :] <= query_pos[:, None]
    keep_mask = visible[:, None, None, :]
    scores = jnp.where(keep_mask, scores, neg_big)
    peak = jnp.max(scores, axis=-1, keepdims=True)
    powers = jnp.where(keep_mask, jnp.exp(scores - peak), 0.0)
    weight = (powers / jnp.maximum(jnp.sum(powers, axis=-1, keepdims=True), 1.0)).astype(
        jnp.bfloat16
    )
    coarse_out = jnp.einsum(
        "qhgn,nhd->qhgd",
        weight,
        summary_values.reshape(summary, kv_dev, HEAD),
        preferred_element_type=jnp.float32,
    )
    member_table = chosen[0]
    start_state = (
        jnp.full((length, kv_dev, per_kv), neg_big, jnp.float32),
        jnp.zeros((length, kv_dev, per_kv), jnp.float32),
        jnp.zeros((length, kv_dev, per_kv, HEAD), jnp.float32),
    )
    kv_count = lax.axis_size("kv")
    block_ids = jnp.arange(kv_count * blocks, dtype=jnp.int32)
    needed = jnp.any(member_table.reshape(-1)[:, None] == block_ids[None, :], axis=0).reshape(
        kv_count, blocks
    )
    others = jnp.arange(kv_count, dtype=jnp.int32) != lax.axis_index("kv")
    needed = needed & others[:, None]
    order_rank = jnp.cumsum(needed.astype(jnp.int32), axis=1) - 1
    in_slot = needed[:, :, None] & (
        order_rank[:, :, None] == jnp.arange(CAP, dtype=jnp.int32)[None, None, :]
    )
    local_block = jnp.sum(
        in_slot.astype(jnp.int32) * jnp.arange(blocks, dtype=jnp.int32)[None, :, None], axis=1
    )
    request = jnp.where(jnp.any(in_slot, axis=1), local_block, -1)
    own_keys = turned_keys.reshape(blocks, BLK, columns)
    own_values = values.reshape(blocks, BLK, columns)
    clipped = jnp.maximum(lax.all_to_all(request, "kv", split_axis=0, concat_axis=0, tiled=True), 0)
    fetched_keys = lax.all_to_all(own_keys[clipped], "kv", split_axis=0, concat_axis=0, tiled=True)
    fetched_values = lax.all_to_all(
        own_values[clipped], "kv", split_axis=0, concat_axis=0, tiled=True
    )
    slot_ids = jnp.where(
        request >= 0, jnp.arange(kv_count, dtype=jnp.int32)[:, None] * blocks + request, -1
    )
    slot_pos = slot_ids[:, :, None] * BLK + jnp.arange(BLK, dtype=jnp.int32)[None, None, :]
    slot_ids = jnp.broadcast_to(slot_ids[:, :, None], slot_pos.shape)
    partial_value = absorb_span(
        start_state,
        turned_query,
        turned_keys,
        values,
        query_pos // BLK,
        query_pos,
        member_table,
        query_pos,
    )
    running_max, weight_sum, weighted = absorb_span(
        partial_value,
        turned_query,
        fetched_keys.reshape(-1, columns),
        fetched_values.reshape(-1, columns),
        slot_ids.reshape(-1),
        slot_pos.reshape(-1),
        member_table,
        query_pos,
    )
    fine_out = weighted / weight_sum[..., None]
    mixed = (
        (gate_cmp[..., None] * coarse_out + gate_slc[..., None] * fine_out)
        .astype(jnp.bfloat16)
        .reshape(length, heads_dev * HEAD)
    )
    summed = lax.psum_scatter(
        jnp.dot(mixed, out_weight, preferred_element_type=jnp.float32),
        "tp",
        scatter_dimension=0,
        tiled=True,
    )
    normed = (
        summed * lax.rsqrt(jnp.mean(summed * summed, axis=-1, keepdims=True) + norm_eps) * out_gain
    )
    return normed[None]


def solution(mesh):
    in_specs = (
        P("dp", "kv", None),
        P(None, "tp"),
        P(None, "tp"),
        P(None, "tp"),
        P(),
        P(),
        P("tp", None),
        P(),
        P("dp", "kv", None),
    )
    out_specs = P("dp", ("kv", "tp"), None)
    return jax.shard_map(
        on_device, mesh=mesh, in_specs=in_specs, out_specs=out_specs, check_vma=False
    )
```

profile of v0, /device:TPU:27, one launch (start us, length us, event | category | flops | bytes accessed | tf_op | source)
XLA Modules:
  0.0 109.5 jit_solution(1949679190152166616)
XLA Ops:
  6.5 0.9 eq.60
  8.9 4.5 %all-to-all-start = ((s32[4,1,2]{2,1,0:T(1,128)}), s32[4,1,2]{2,1,0:T(1,128)}, u32[]{:S(2)}, u32[]{:S(2)}) async-start(s32[4,1,2]{2,1,0:T(1,128)} %copy.66), calls=%async_computation | async-start | bytes 4096 | tf_op jit(solution)/shard_map/all_to_all | solution.py:212
  14.1 2.5 %convolution_convert_fusion = bf16[256,384]{1,0:T(8,128)(2,1)S(1)} fusion(bf16[2048,384]{1,0:T(8,128)(2,1)} %param.10, bf16[1,256,2048]{2,1,0:T(8,128)(2,1)} %param.9), kind=kOutput, calls=%fused_computation.22 | convolution fusion | flops 402751488 | bytes 2818048 | tf_op jit(solution)/shard_map/dot_general | solution.py:136
  16.9 1.5 %convolution_convert_fusion.2 = bf16[256,128]{1,0:T(8,128)(2,1)S(1)} fusion(bf16[2048,128]{1,0:T(8,128)(2,1)} %param.12, bf16[1,256,2048]{2,1,0:T(8,128)(2,1)S(1)} %copy-done.1), kind=kOutput, calls=%fused_computation.30 | convolution fusion | flops 134250496 | bytes 1638400 | tf_op jit(solution)/shard_map/dot_general | solution.py:138
  19.3 0.8 bitcast_and_fusion
  20.8 1.5 %convolution_convert_fusion.1 = bf16[256,128]{0,1:T(8,128)(2,1)S(1)} fusion(bf16[2048,128]{1,0:T(8,128)(2,1)} %param.11, bf16[1,256,2048]{2,1,0:T(8,128)(2,1)S(1)} %copy-done.1), kind=kOutput, calls=%fused_computation.29 | convolution fusion | flops 134250496 | bytes 1638400 | tf_op jit(solution)/shard_map/dot_general | solution.py:137
  24.6 1.6 %copy.65 = bf16[256,2,64]{2,1,0:T(2,128)(2,1)} copy(bf16[256,2,64]{0,2,1:T(8,128)(2,1)} %maximum_convert_fusion) | data formatting | bytes 131072 | tf_op jit(solution)/shard_map/convert_element_type | solution.py:32
  26.2 1.6 %convert_element_type.88 = bf16[8,32,128]{2,1,0:T(8,128)(2,1)} reshape(bf16[256,2,64]{2,1,0:T(2,128)(2,1)} %copy.65) | data formatting | bytes 131072 | tf_op jit(solution)/shard_map/convert_element_type | solution.py:32
  28.5 1.0 copy.58
  29.6 1.3 %fusion.21 = f32[256,24]{0,1:T(8,128)S(1)} fusion(bf16[2048,24]{0,1:T(8,128)(2,1)} %param.13, bf16[1,256,2048]{2,1,0:T(8,128)(2,1)S(1)} %copy-done.1), kind=kOutput, calls=%fused_computation.34 | convolution fusion | flops 25165824 | bytes 1171456 | tf_op jit(solution)/shard_map/dot_general | solution.py:139
  32.2 0.9 reshape.460
  33.4 8.3 %all_gather.7 = bf16[32,128]{1,0:T(8,128)(2,1)S(1)} all-gather(bf16[8,128]{1,0:T(8,128)(2,1)S(1)} %reshape.461), channel_id=1, replica_groups=mesh['dp'=4,'kv'=4,'tp'=2] {'kv'}, dimensions={0}, use_global_device_ids=true | all-gather | bytes 10240 | tf_op jit(solution)/shard_map/all_gather | solution.py:165
  42.7 2.0 %fusion.49 = (f32[256,2,3]{0,2,1:T(4,128)}, f32[256,2,3,256]{0,3,2,1:T(8,128)S(1)}) fusion(bf16[256,2,3,32]{0,3,2,1:T(8,128)(2,1)} %bitcast.121, bf16[256,2,3,32]{0,3,2,1:T(8,128)(2,1)} %bitcast.119, pred[256,256]{0,1:T(8,128)(4,1)S(1)} %copy.58, bf16[256,2,32]{0,2,1:T(8,128)(2,1)} %copy-done.7, bf16[256,2,32]{0,2,1:T(8,128)(2,1)} %copy-done.6), kind=kOutput, calls=%fused_computation.114 | convolution fusion | flops 52034048 | bytes 1906688 | tf_op jit(solution)/shard_map/qhgd,khd->qhgk/dot_general | solution.py:52
  44.7 1.2 %maximum_reduce_fusion = s32[4,2]{1,0:T(4,128)} fusion(s32[4,1,2]{2,1,0:T(1,128)} %all-to-all-done), kind=kLoop, calls=%fused_computation.87 | loop fusion | flops 8 | bytes 64 | tf_op jit(solution)/shard_map/max | solution.py:212
  45.9 1.3 %reshape.474 = s32[8]{0:T(128)} reshape(s32[4,2]{1,0:T(4,128)} %maximum_reduce_fusion) | data formatting | bytes 64 | tf_op jit(solution)/shard_map/max | solution.py:212
  47.2 1.2 %pad_clamp_fusion = s32[1024]{0:T(1024)} fusion(s32[8]{0:T(128)} %reshape.474), kind=kLoop, calls=%fused_computation.75 | loop fusion | flops 1024 | bytes 4128 | tf_op jit(solution)/shard_map/gather | solution.py:213
  48.4 2.1 %gather_fusion = bf16[8,32,128]{2,1,0:T(8,128)(2,1)} fusion(bf16[8,32,128]{2,1,0:T(8,128)(2,1)} %convert_element_type.88, s32[1024]{0:T(1024)} %pad_clamp_fusion), kind=kCustom, calls=%fused_computation | custom fusion | bytes 131104 | tf_op jit(solution)/shard_map/gather | solution.py:213
  50.6 5.1 %all-to-all-start.1 = ((bf16[4,2,32,128]{3,2,1,0:T(8,128)(2,1)}), bf16[4,2,32,128]{3,2,1,0:T(8,128)(2,1)}, u32[]{:S(2)}, u32[]{:S(2)}) async-start(bf16[4,2,32,128]{3,2,1,0:T(8,128)(2,1)} %bitcast.115), calls=%async_computation.1 | async-start | bytes 131072 | tf_op jit(solution)/shard_map/all_to_all | solution.py:213
  55.7 0.8 multiply_reduce_fusion.2
  56.5 0.8 reshape.458
  57.2 8.7 %all_gather.6 = bf16[32,128]{1,0:T(8,128)(2,1)S(1)} all-gather(bf16[8,128]{1,0:T(8,128)(2,1)S(1)} %reshape.458), channel_id=1, replica_groups=mesh['dp'=4,'kv'=4,'tp'=2] {'kv'}, dimensions={0}, use_global_device_ids=true | all-gather | bytes 10240 | tf_op jit(solution)/shard_map/all_gather | solution.py:166
  66.6 1.3 %gather_fusion.1 = bf16[8,32,128]{2,1,0:T(8,128)(2,1)} fusion(bf16[8,32,128]{2,1,0:T(8,128)(2,1)S(1)} %bitcast.111, s32[1024]{0:T(1024)} %pad_clamp_fusion), kind=kCustom, calls=%fused_computation.1 | custom fusion | bytes 131104 | tf_op jit(solution)/shard_map/gather | solution.py:215
  67.9 4.5 %all-to-all-start.2 = ((bf16[4,2,32,128]{3,2,1,0:T(8,128)(2,1)}), bf16[4,2,32,128]{3,2,1,0:T(8,128)(2,1)S(1)}, u32[]{:S(2)}, u32[]{:S(2)}) async-start(bf16[4,2,32,128]{3,2,1,0:T(8,128)(2,1)} %bitcast.36), calls=%async_computation.2 | async-start | bytes 131072 | tf_op jit(solution)/shard_map/all_to_all | solution.py:214
  72.5 0.9 reshape_reshape.7
  73.4 1.3 %fusion.50 = (f32[256,2,3]{0,2,1:T(4,128)S(1)}, f32[256,2,3,256]{0,3,2,1:T(8,128)S(1)}) fusion(bf16[256,2,3,32]{0,3,2,1:T(8,128)(2,1)} %bitcast.122, bf16[256,2,3,32]{0,3,2,1:T(8,128)(2,1)} %bitcast.120, bf16[256,2,64,1]{2,1,0,3:T(2,128)(2,1)S(1)} %bitcast.118, pred[256,256]{0,1:T(8,128)(4,1)S(1)} %copy-done.4), kind=kOutput, calls=%fused_computation.115 | convolution fusion | flops 51902976 | bytes 1906688 | tf_op jit(solution)/shard_map/qhgd,khd->qhgk/dot_general | solution.py:52
  75.9 1.1 %fusion.11 = f32[256,2,3,64]{0,3,2,1:T(8,128)} fusion(bf16[256,2,64,1]{0,2,3,1:T(8,128)(2,1)S(1)} %bitcast.114, f32[256,2,3,256]{0,3,2,1:T(8,128)S(1)} %get-tuple-element.30, f32[256,2,3]{0,2,1:T(4,128)S(1)} %get-tuple-element.23, pred[256,256]{0,1:T(8,128)(4,1)S(1)} %copy.58, f32[256,2,3]{0,2,1:T(4,128)S(1)} %get-tuple-element.8, ...), kind=kOutput, calls=%fused_computation.20 | convolution fusion | flops 51707904 | bytes 2115584 | tf_op jit(solution)/shard_map/qhgk,khd->qhgd/dot_general | solution.py:61
  77.2 1.9 %fusion.9 = f32[256,2,3,64]{0,3,2,1:T(8,128)S(1)} fusion(f32[256,2,3,64]{0,3,2,1:T(8,128)} %fusion.11, f32[256,2,3,256]{0,3,2,1:T(8,128)} %copy-done.3, f32[256,2,3]{0,2,1:T(4,128)S(1)} %get-tuple-element.22, pred[256,256]{0,1:T(8,128)(4,1)S(1)} %copy-done.4, f32[256,2,3]{0,2,1:T(4,128)S(1)} %get-tuple-element.7, f32[256,2,3]{0,2,1:T(4,128)S(1)} %copy-done.16, ...), kind=kOutput, calls=%fused_computation.18 | convolution fusion | flops 51806208 | bytes 2508800 | tf_op jit(solution)/shard_map/qhgk,khd->qhgd/dot_general | solution.py:61
  79.1 1.3 %fusion.13 = bf16[256,2,3,64]{0,3,2,1:T(8,128)(2,1)S(1)} fusion(f32[256,2,3,64]{0,3,2,1:T(8,128)S(1)} %fusion.9, f32[256,2,3]{0,2,1:T(4,128)S(1)} %copy-done.15, f32[256,2,3]{0,2,1:T(4,128)S(1)} %copy-done.17, f32[256,2,3,32]{0,3,2,1:T(8,128)} %copy-done.5, pred[256,32]{0,1:T(8,128)(4,1)S(1)} %copy-done.9, bf16[32,2,64,1]{2,1,0,3:T(2,128)(2,1)S(1)} %bitcast.126), kind=kOutput, calls=%fused_computation.23 | convolution fusion | flops 6784543 | bytes 815104 | tf_op jit(solution)/shard_map/qhgn,nhd->qhgd/dot_general | solution.py:183
  80.4 2.1 %fusion.52 = f32[256,2048]{1,0:T(8,128)} fusion(bf16[256,384]{0,1:T(8,128)(2,1)S(1)} %bitcast.116, bf16[384,2048]{1,0:T(8,128)(2,1)S(1)} %copy-done), kind=kOutput, calls=%fused_computation.117 | convolution fusion | flops 402653184 | bytes 3866624 | tf_op jit(solution)/shard_map/dot_general | solution.py:249
  82.5 17.4 %reduce-scatter.2.cloned.1.call-done = f32[128,2048]{1,0:T(8,128)} async-done(((f32[256,2048]{1,0:T(8,128)}), f32[128,2048]{1,0:T(8,128)}) %reduce-scatter.2.cloned.1.call-update) | async-done | bytes 1048592 | tf_op jit(solution)/shard_map/reduce_scatter | solution.py:248
  100.0 1.5 %multiply_reduce_fusion = f32[128]{0:T(128)S(1)} fusion(f32[128,2048]{1,0:T(8,128)} %reduce-scatter.2.cloned.1.call-done), kind=kLoop, calls=%fused_computation.37 | loop fusion | flops 524160 | bytes 1049088 | tf_op jit(solution)/shard_map/reduce_sum | solution.py:255
  101.5 1.1 %multiply_bitcast_fusion = f32[1,128,2048]{2,1,0:T(8,128)} fusion(f32[128,2048]{1,0:T(8,128)S(1)} %copy-done.2, f32[2048]{0:T(1024)S(1)} %copy-done.14, f32[128]{0:T(128)S(1)} %add_rsqrt_fusion), kind=kLoop, calls=%fused_computation.36 | loop fusion | flops 524288 | bytes 2105856 | tf_op jit(solution)/shard_map/broadcast_in_dim | solution.py:257
  (98 shorter events, 11.4 us)
Async XLA Ops:
  6.5 73.9 %copy-start = (bf16[384,2048]{1,0:T(8,128)(2,1)S(1)}, bf16[384,2048]{1,0:T(8,128)(2,1)}, u32[]{:S(2)}) copy-start(bf16[384,2048]{1,0:T(8,128)(2,1)} %param.15) | copy-start | bytes 4718596
  8.9 35.8 %all-to-all-start = ((s32[4,1,2]{2,1,0:T(1,128)}), s32[4,1,2]{2,1,0:T(1,128)}, u32[]{:S(2)}, u32[]{:S(2)}) async-start(s32[4,1,2]{2,1,0:T(1,128)} %copy.66), calls=%async_computation | async-start | bytes 4096 | tf_op jit(solution)/shard_map/all_to_all | solution.py:212
  14.1 2.8 %copy-start.1 = (bf16[1,256,2048]{2,1,0:T(8,128)(2,1)S(1)}, bf16[1,256,2048]{2,1,0:T(8,128)(2,1)}, u32[]{:S(2)}) copy-start(bf16[1,256,2048]{2,1,0:T(8,128)(2,1)} %param.9) | copy-start | bytes 3145732
  16.6 2.5 %copy-start.13 = (s32[1,8,16]{2,1,0:T(8,128)S(1)}, s32[1,8,16]{2,1,0:T(8,128)}, u32[]{:S(2)}) copy-start(s32[1,8,16]{2,1,0:T(8,128)} %param.17) | copy-start | bytes 1540
  23.1 9.0 %copy-start.18 = (s32[32]{0:T(128)S(1)}, s32[32]{0:T(128)}, u32[]{:S(2)}) copy-start(s32[32]{0:T(128)} %multiply_add_fusion.2) | copy-start | bytes 388
  23.3 0.6 copy-start.6
  23.3 0.6 copy-start.7
  28.5 4.6 %copy-start.10 = (f32[2,32,64]{2,1,0:T(8,128)S(1)}, f32[2,32,64]{2,1,0:T(8,128)}, u32[]{:S(2)}) copy-start(f32[2,32,64]{2,1,0:T(8,128)} %param.14) | copy-start | bytes 49156
  32.2 10.5 %copy-start.8 = (pred[256,32]{0,1:T(8,128)(4,1)}, pred[256,32]{0,1:T(8,128)(4,1)S(1)}, u32[]{:S(2)}) copy-start(pred[256,32]{0,1:T(8,128)(4,1)S(1)} %broadcast_compare_fusion) | copy-start | bytes 24580
  42.0 0.7 copy-start.5
  42.0 31.4 %copy-start.4 = (pred[256,256]{0,1:T(8,128)(4,1)S(1)}, pred[256,256]{0,1:T(8,128)(4,1)}, u32[]{:S(2)}) copy-start(pred[256,256]{0,1:T(8,128)(4,1)} %copy.64) | copy-start | bytes 196612
  50.6 17.4 %all-to-all-start.1 = ((bf16[4,2,32,128]{3,2,1,0:T(8,128)(2,1)}), bf16[4,2,32,128]{3,2,1,0:T(8,128)(2,1)}, u32[]{:S(2)}, u32[]{:S(2)}) async-start(bf16[4,2,32,128]{3,2,1,0:T(8,128)(2,1)} %bitcast.115), calls=%async_computation.1 | async-start | bytes 131072 | tf_op jit(solution)/shard_map/all_to_all | solution.py:213
  56.4 18.3 %copy-start.11 = (f32[256,2,3]{0,2,1:T(4,128)S(1)}, f32[256,2,3]{0,2,1:T(4,128)}, u32[]{:S(2)}) copy-start(f32[256,2,3]{0,2,1:T(4,128)} %get-tuple-element.29) | copy-start | bytes 18436
  67.9 9.1 %all-to-all-start.2 = ((bf16[4,2,32,128]{3,2,1,0:T(8,128)(2,1)}), bf16[4,2,32,128]{3,2,1,0:T(8,128)(2,1)S(1)}, u32[]{:S(2)}, u32[]{:S(2)}) async-start(bf16[4,2,32,128]{3,2,1,0:T(8,128)(2,1)} %bitcast.36), calls=%async_computation.2 | async-start | bytes 131072 | tf_op jit(solution)/shard_map/all_to_all | solution.py:214
  72.5 27.5 %reduce-scatter.2.cloned.1.call-start = ((), (), s32[]{:S(2)}) async-start(), calls=%async_computation.4 | async-start | bytes 3145728 | tf_op jit(solution)/shard_map/reduce_scatter | solution.py:248
  74.7 1.2 %copy-start.3 = (f32[256,2,3,256]{0,3,2,1:T(8,128)}, f32[256,2,3,256]{0,3,2,1:T(8,128)S(1)}, u32[]{:S(2)}) copy-start(f32[256,2,3,256]{0,3,2,1:T(8,128)S(1)} %get-tuple-element.32) | copy-start | bytes 4718596
  75.9 1.3 %copy-start.16 = (f32[256,2,3]{0,2,1:T(4,128)S(1)}, f32[256,2,3]{0,2,1:T(4,128)}, u32[]{:S(2)}) copy-start(f32[256,2,3]{0,2,1:T(4,128)} %mul.221) | copy-start | bytes 18436
  77.2 1.9 %copy-start.9 = (pred[256,32]{0,1:T(8,128)(4,1)S(1)}, pred[256,32]{0,1:T(8,128)(4,1)}, u32[]{:S(2)}) copy-start(pred[256,32]{0,1:T(8,128)(4,1)} %copy-done.8) | copy-start | bytes 24580
  77.2 1.9 %copy-start.12 = (bf16[32,2,64]{2,1,0:T(2,128)(2,1)S(1)}, bf16[32,2,64]{2,1,0:T(2,128)(2,1)}, u32[]{:S(2)}) copy-start(bf16[32,2,64]{2,1,0:T(2,128)(2,1)} %reshape.459) | copy-start | bytes 24580
  77.2 1.9 %copy-start.15 = (f32[256,2,3]{0,2,1:T(4,128)S(1)}, f32[256,2,3]{0,2,1:T(4,128)}, u32[]{:S(2)}) copy-start(f32[256,2,3]{0,2,1:T(4,128)} %mul.212) | copy-start | bytes 18436
  77.2 1.9 %copy-start.17 = (f32[256,2,3]{0,2,1:T(4,128)S(1)}, f32[256,2,3]{0,2,1:T(4,128)}, u32[]{:S(2)}) copy-start(f32[256,2,3]{0,2,1:T(4,128)} %broadcast_maximum_fusion.1) | copy-start | bytes 18436
  82.5 19.0 %copy-start.14 = (f32[2048]{0:T(1024)S(1)}, f32[2048]{0:T(1024)}, u32[]{:S(2)}) copy-start(f32[2048]{0:T(1024)} %param.16) | copy-start | bytes 24580
  100.0 1.5 %copy-start.2 = (f32[128,2048]{1,0:T(8,128)S(1)}, f32[128,2048]{1,0:T(8,128)}, u32[]{:S(2)}) copy-start(f32[128,2048]{1,0:T(8,128)} %reduce-scatter.2.cloned.1.call-done) | copy-start | bytes 3145732
Sparse Core Ops, SparseCore 0:
  82.7 17.2 reduce-scatter.1
where the time goes:
time: 112 us; the launch traced here: 109 us
  local copies, waits for them, and re-layouts  19 us (17%)
  waiting for transfers between devices  17.5 us (16%)
  blocking collectives  17.1 us (15%)
  matrix products  16.6 us (15%)
  starting transfers between devices  14.2 us (13%)
  between operations  13.8 us (12%)
  other arithmetic  11.3 us (10%)
    reduce_scatter x1, waiting for transfers between devices, on_device(): lax.psum_scatter(jnp.dot(mixed, out_weight, preferred_element_type=jnp.fl...  17.4 us
    all_gather x1, blocking collectives, on_device(): lax.all_gather(packed_values, 'kv', axis=0, tiled=True)  8.74 us
    all_gather x1, blocking collectives, on_device(): lax.all_gather(packed_keys, 'kv', axis=0, tiled=True)  8.34 us
    all_to_all x1, starting transfers between devices, on_device(): lax.all_to_all(own_keys[clipped], 'kv', split_axis=0, concat_axis=0, tile...  5.12 us
    all_to_all x1, starting transfers between devices, on_device(): lax.all_to_all(own_values[clipped], 'kv', split_axis=0, concat_axis=0, ti...  4.53 us
    all_to_all x1, starting transfers between devices, on_device(): lax.all_to_all(request, 'kv', split_axis=0, concat_axis=0, tiled=True)  4.53 us
    dot_general x2, matrix products, absorb(): jnp.einsum('qhgd,khd->qhgk', queries, key_part, preferred_element_type=jn...  3.31 us
    convert_element_type x2, local copies, waits for them, and re-layouts, rotate(): return turned.astype(jnp.bfloat16)  3.26 us
  transfers between devices with their start and end apart: 4, of which 1 were waited for; matrix products, arithmetic and copies ran while one was open for 27% of the time, Pallas kernels for 0%

commit v1 on v0

v1 whole, which is shorter than its diff:
```python
import functools

import numpy as np
import jax
import jax.numpy as jnp
from jax import lax
from jax.experimental import pallas as pl
from jax.experimental.pallas import tpu as pltpu
from jax.sharding import PartitionSpec as P

HEAD = 64
BLK = 32
CAP = 2
NEG = -1e30
ROPE_BASE = 500000.0
EPS = 1e-06
F32 = jnp.float32
BF = jnp.bfloat16
ANY = pl.BlockSpec(memory_space=pl.ANY)


def mm(a, b):
    return jnp.dot(a, b, preferred_element_type=F32)


def mm_t(a, b):
    return lax.dot_general(a, b, (((1,), (1,)), ((), ())), preferred_element_type=F32)


def iota(shape, dim):
    return lax.broadcasted_iota(jnp.int32, shape, dim)


def rope_table(kvn, length):
    half = HEAD // 2
    inverse = ROPE_BASE ** (-np.arange(half) * (2.0 / HEAD))
    angles = np.arange(kvn * length)[None, :] * inverse[:, None]
    table = np.stack([np.cos(angles), np.sin(angles)]).astype(np.float32)
    return table.reshape(2, half, kvn, length).transpose(2, 0, 1, 3).copy()


def kernel(
    kvn,
    tpn,
    tok_h,
    wq_h,
    wk_h,
    wv_h,
    wg_h,
    cw_h,
    wo_h,
    gain_h,
    chosen_h,
    tab_h,
    out_h,
    tok,
    wkv,
    wq,
    wg,
    cw,
    wo,
    wo2,
    gain,
    chosen,
    tab,
    reqs,
    reqin,
    maskb,
    tkv,
    vt,
    coarse,
    blk_out,
    blks,
    qp,
    qt,
    gt,
    mixt,
    mix_own,
    mix_out,
    mix_in,
    acc,
    lsem,
    osem,
    req_s,
    req_r,
    co_s,
    co_r,
    bl_s,
    bl_r,
    wo_s,
    wo_r,
    mx_s,
    mx_r,
):
    dp = lax.axis_index("dp")
    me = lax.axis_index("kv")
    tp = lax.axis_index("tp")
    length, width = tok.shape
    cols = wkv.shape[1] // 2
    kv_dev = cols // HEAD
    heads = wq.shape[1] // HEAD
    per_kv = heads // kv_dev
    nb = length // BLK
    total_blocks = kvn * nb
    rows_out = length // tpn
    slot_rows = CAP * BLK

    def local(src, dst, index):
        return pltpu.make_async_copy(src, dst, lsem.at[index])

    loads = [
        local(chosen_h.at[0], chosen, 0),
        local(tab_h.at[me], tab, 1),
        local(tok_h.at[0], tok, 2),
        local(wk_h, wkv.at[:, 0:cols], 3),
        local(wv_h, wkv.at[:, cols : 2 * cols], 4),
        local(cw_h, cw, 5),
        local(wq_h, wq, 6),
        local(wg_h, wg, 7),
        local(wo_h, wo, 8),
        local(gain_h, gain, 9),
    ]
    for load in loads:
        load.start()

    barrier = pltpu.get_barrier_semaphore()
    for d in range(1, kvn):
        peer = lax.rem(me + d, kvn)
        pl.semaphore_signal(
            barrier, inc=1, device_id=(dp, peer, tp), device_id_type=pl.DeviceIdType.MESH
        )
    other = (dp, me, tpn - 1 - tp)
    pl.semaphore_signal(barrier, inc=1, device_id=other, device_id_type=pl.DeviceIdType.MESH)

    def remote(src, dst, send, recv, target):
        return pltpu.make_async_remote_copy(
            src_ref=src,
            dst_ref=dst,
            send_sem=send,
            recv_sem=recv,
            device_id=target,
            device_id_type=pl.DeviceIdType.MESH,
        )

    def req_copy(d):
        return remote(
            reqs.at[d], reqin.at[d], req_s.at[d], req_r.at[d], (dp, lax.rem(me - d + kvn, kvn), tp)
        )

    def coarse_copy(d):
        return remote(
            coarse.at[0], coarse.at[d], co_s.at[d], co_r.at[d], (dp, lax.rem(me + d, kvn), tp)
        )

    def block_copy(d):
        return remote(
            blk_out.at[d - 1],
            blks.at[d - 1],
            bl_s.at[d],
            bl_r.at[d],
            (dp, lax.rem(me + d, kvn), tp),
        )

    weight_copy = remote(wo_h, wo2, wo_s, wo_r, other)
    mix_copy = remote(mix_out, mix_in, mx_s, mx_r, other)

    for d in range(1, kvn):

        @pl.when(me < d)
        def _():
            blks[d - 1] = jnp.zeros(blks.shape[1:], BF)
            coarse[d] = jnp.zeros(coarse.shape[1:], F32)

    loads[0].wait()
    listed = chosen[...]
    lane_blk = iota((nb, total_blocks), 1)
    hit = jnp.zeros((nb, total_blocks), F32)
    for t in range(listed.shape[1]):
        hit = jnp.where(listed[:, t : t + 1] == lane_blk, 1.0, hit)
    needed = jnp.max(hit, axis=0, keepdims=True)
    gi = iota((total_blocks, total_blocks), 0)
    gj = iota((total_blocks, total_blocks), 1)
    before = jnp.where((gi // nb == gj // nb) & (gi < gj), 1.0, 0.0).astype(BF)
    rank = mm(jnp.broadcast_to(needed, (8, total_blocks)).astype(BF), before)[0:1]
    ra = iota((kvn * 8, total_blocks), 0)
    ja = iota((kvn * 8, total_blocks), 1)
    pick = jnp.where(
        (needed > 0.5)
        & (rank == (ra % 8).astype(F32))
        & (ra % 8 < CAP)
        & (ja // nb == me - ra // 8),
        1.0,
        0.0,
    )
    wanted = jnp.sum(pick * ((ja % nb) + 1).astype(F32), axis=1, keepdims=True) - 1.0
    reqs[...] = jnp.broadcast_to(wanted, (kvn * 8, 128)).reshape(kvn, 8, 128)

    pl.semaphore_wait(barrier, kvn)
    for d in range(1, kvn):

        @pl.when(me >= d)
        def _():
            req_copy(d).start()

    weight_copy.start()
    spread = jnp.where(iota((nb, length), 1) // BLK == iota((nb, length), 0), 1.0, 0.0)
    member = mm(mm_t(pick, hit), spread)
    maskb[...] = jnp.where(member > 0.5, 0.0, NEG)

    loads[1].wait()
    cos_t = tab[0]
    sin_t = tab[1]
    cos_n = jnp.concatenate([cos_t, cos_t] * kv_dev, axis=0).T
    sin_n = jnp.concatenate([-sin_t, sin_t] * kv_dev, axis=0).T

    for index in (2, 3, 4, 5):
        loads[index].wait()
    both = mm(tok[...], wkv[...]).astype(BF)
    tkv[:, cols : 2 * cols] = both[:, cols : 2 * cols]
    both = both.astype(F32)
    key_f = both[:, 0:cols]
    val_f = both[:, cols : 2 * cols]

    def compress(x, index):
        weight = jnp.concatenate([cw[index]] * kv_dev, axis=1)
        packed = jnp.sum(x.reshape(nb, BLK, cols) * weight[None], axis=1)
        return packed.astype(BF).astype(F32)

    coarse[0, 0:nb] = compress(key_f, 0)
    coarse[0, nb : 2 * nb] = compress(val_f, 1)
    for d in range(1, kvn):

        @pl.when(me + d < kvn)
        def _():
            coarse_copy(d).start()

    half = HEAD // 2
    low = iota((length, cols), 1) % HEAD < half
    swapped = jnp.where(low, pltpu.roll(key_f, cols - half, 1), pltpu.roll(key_f, half, 1))
    tkv[:, 0:cols] = (key_f * cos_n + swapped * sin_n).astype(BF)

    si = iota((slot_rows, length), 0)
    sj = iota((slot_rows, length), 1)
    for d in range(1, kvn):

        @pl.when(me + d < kvn)
        def _():
            req_copy(d).wait_recv()
            tile = reqin[d]
            ask = jnp.concatenate(
                [jnp.broadcast_to(tile[s : s + 1], (BLK, 128)) for s in range(CAP)], axis=0
            )
            ask = jnp.concatenate([ask] * (length // 128), axis=1)
            chooser = jnp.where(
                (ask == (sj // BLK).astype(F32)) & (si % BLK == sj % BLK), 1.0, 0.0
            ).astype(BF)
            sent = mm(chooser, tkv[...]).astype(BF)
            blk_out[d - 1, 0:slot_rows] = sent[:, 0:cols]
            blk_out[d - 1, slot_rows : 2 * slot_rows] = sent[:, cols : 2 * cols]
            block_copy(d).start()

    vt[...] = val_f.T.astype(BF)

    loads[6].wait()
    scale = HEAD ** (-0.5)
    query_t = mm(tok[...], wq[...]).astype(BF).astype(F32).T * scale
    qp[...] = query_t.astype(BF)
    for h in range(heads):
        first = query_t[h * HEAD : h * HEAD + half]
        second = query_t[h * HEAD + half : (h + 1) * HEAD]
        qt[h * HEAD : h * HEAD + half] = (first * cos_t - second * sin_t).astype(BF)
        qt[h * HEAD + half : (h + 1) * HEAD] = (second * cos_t + first * sin_t).astype(BF)
    loads[7].wait()
    gates = jax.nn.sigmoid(mm_t(wg[...], tok[...]))
    for branch in range(2):
        mine = jnp.zeros((heads, length), F32)
        for t in range(tpn):
            row = (branch * tpn + t) * heads
            mine = jnp.where(tp == t, gates[row : row + heads], mine)
        gt[branch * heads : (branch + 1) * heads] = mine

    for d in range(1, kvn):

        @pl.when(me >= d)
        def _():
            coarse_copy(d).wait_recv()

    coarse_k = coarse[:, 0:nb].reshape(kvn * nb, cols)
    coarse_vt = coarse[:, nb : 2 * nb].reshape(kvn * nb, cols).T
    ck = [coarse_k[:, k * HEAD : (k + 1) * HEAD].astype(BF) for k in range(kv_dev)]
    cvt = [coarse_vt[k * HEAD : (k + 1) * HEAD].astype(BF) for k in range(kv_dev)]

    for d in range(1, kvn):

        @pl.when(me >= d)
        def _():
            block_copy(d).wait_recv()

    far = (kvn - 1) * slot_rows
    far_k = blks[:, 0:slot_rows].reshape(far, cols)
    far_vt = blks[:, slot_rows : 2 * slot_rows].reshape(far, cols).astype(F32).T.astype(BF)
    kr = [far_k[:, k * HEAD : (k + 1) * HEAD] for k in range(kv_dev)]
    vr = [far_vt[k * HEAD : (k + 1) * HEAD] for k in range(kv_dev)]

    n = rows_out
    dk = iota((n, n), 0)
    dq = iota((n, n), 1)
    near_bias = jnp.where((dk // BLK == dq // BLK) & (dk <= dq), 0.0, NEG)
    cr = iota((kvn * nb, n), 0)
    cb = (me - cr // nb) * nb + cr % nb

    def attend(chunk):
        start = pl.multiple_of(chunk * n, n)
        here = pl.ds(start, n)
        far_bias = jnp.concatenate(
            [
                jnp.broadcast_to(maskb[d * 8 + s : d * 8 + s + 1, here], (BLK, n))
                for d in range(1, kvn)
                for s in range(CAP)
            ],
            axis=0,
        )
        pos = me * length + start + iota((kvn * nb, n), 1)
        seen = (cb >= 0) & ((cb + 1) * BLK - 1 <= pos)
        near_k = tkv[here, 0:cols]
        kd = [near_k[:, k * HEAD : (k + 1) * HEAD] for k in range(kv_dev)]
        for h in range(heads):
            k = h // per_kv
            rows = slice(h * HEAD, (h + 1) * HEAD)
            sc = jnp.where(seen, mm(ck[k], qp[rows, here]), NEG)
            peak = jnp.max(sc, axis=0, keepdims=True)
            pw = jnp.where(seen, jnp.exp(sc - peak), 0.0)
            weight = pw / jnp.maximum(jnp.sum(pw, axis=0, keepdims=True), 1.0)
            coarse_out = mm(cvt[k], weight.astype(BF))
            query = qt[rows, here]
            sf = mm(kr[k], query) + far_bias
            sn = mm(kd[k], query) + near_bias
            top = jnp.maximum(
                jnp.max(sf, axis=0, keepdims=True), jnp.max(sn, axis=0, keepdims=True)
            )
            pf = jnp.exp(sf - top)
            pn = jnp.exp(sn - top)
            norm = jnp.sum(pf, axis=0, keepdims=True) + jnp.sum(pn, axis=0, keepdims=True)
            fine = mm(vr[k], pf.astype(BF)) + mm(
                vt[k * HEAD : (k + 1) * HEAD, here], pn.astype(BF)
            )
            g_coarse = gt[h : h + 1, here]
            g_fine = gt[heads + h : heads + h + 1, here]
            mixt[rows] = g_coarse * coarse_out + fine * (g_fine / norm)
        return mixt[...].T.astype(BF)

    mix_out[...] = attend(tpn - 1 - tp)
    mix_copy.start()
    mix_own[...] = attend(tp)
    loads[8].wait()
    step = 512
    for c in range(0, width, step):
        acc[:, c : c + step] = mm(mix_own[...], wo[:, c : c + step])
    loads[9].wait()
    weight_copy.wait_recv()
    mix_copy.wait_recv()
    square = jnp.zeros((n, 1), F32)
    for c in range(0, width, step):
        part = acc[:, c : c + step] + mm(mix_in[...], wo2[:, c : c + step])
        acc[:, c : c + step] = part
        square = square + jnp.sum(part * part, axis=1, keepdims=True)
    factor = lax.rsqrt(square * (1.0 / width) + EPS)
    pieces = 4
    span = n // pieces
    stores = []
    for i in range(pieces):
        rows = slice(i * span, (i + 1) * span)
        acc[rows] = acc[rows] * factor[rows] * gain[...]
        store = pltpu.make_async_copy(acc.at[pl.ds(i * span, span)], out_h.at[0, pl.ds(i * span, span)], osem.at[i])
        store.start()
        stores.append(store)
    for store in stores:
        store.wait()
    weight_copy.wait_send()
    mix_copy.wait_send()
    for d in range(1, kvn):

        @pl.when(me >= d)
        def _():
            req_copy(d).wait_send()

        @pl.when(me + d < kvn)
        def _():
            coarse_copy(d).wait_send()
            block_copy(d).wait_send()


def on_device(kvn, tpn, tokens, wq, wk, wv, wg, cw, wo, gain, chosen):
    length, width = tokens.shape[1:]
    cols = wk.shape[1]
    qcols = wq.shape[1]
    table = jnp.asarray(rope_table(kvn, length))
    nb = length // BLK
    rows_out = length // tpn
    V = pltpu.VMEM
    dma = pltpu.SemaphoreType.DMA
    scratch = [
        V((length, width), BF),
        V((width, 2 * cols), BF),
        V((width, qcols), BF),
        V((wg.shape[1], width), BF),
        V(cw.shape, F32),
        V(wo.shape, BF),
        V(wo.shape, BF),
        V((1, width), F32),
        V(chosen.shape[1:], jnp.int32),
        V(table.shape[1:], F32),
        V((kvn, 8, 128), F32),
        V((kvn, 8, 128), F32),
        V((kvn * 8, length), F32),
        V((length, 2 * cols), BF),
        V((cols, length), BF),
        V((kvn, 2 * nb, cols), F32),
        V((kvn - 1, 2 * CAP * BLK, cols), BF),
        V((kvn - 1, 2 * CAP * BLK, cols), BF),
        V((qcols, length), BF),
        V((qcols, length), BF),
        V((wg.shape[1] // tpn, length), F32),
        V((qcols, rows_out), F32),
        V((rows_out, qcols), BF),
        V((rows_out, qcols), BF),
        V((rows_out, qcols), BF),
        V((rows_out, width), F32),
        dma((10,)),
        dma((4,)),
        dma((kvn,)),
        dma((kvn,)),
        dma((kvn,)),
        dma((kvn,)),
        dma((kvn,)),
        dma((kvn,)),
        dma,
        dma,
        dma,
        dma,
    ]
    return pl.pallas_call(
        functools.partial(kernel, kvn, tpn),
        out_shape=jax.ShapeDtypeStruct((1, rows_out, width), F32),
        in_specs=[ANY] * 10,
        out_specs=ANY,
        scratch_shapes=scratch,
        compiler_params=pltpu.CompilerParams(
            collective_id=0, has_side_effects=True, vmem_limit_bytes=67043328
        ),
    )(tokens, wq, wk, wv, wg.T, cw, wo, gain.reshape(1, width), chosen, table)


def solution(mesh):
    in_specs = (
        P("dp", "kv", None),
        P(None, "tp"),
        P(None, "tp"),
        P(None, "tp"),
        P(),
        P(),
        P("tp", None),
        P(),
        P("dp", "kv", None),
    )
    return jax.shard_map(
        functools.partial(on_device, mesh.shape["kv"], mesh.shape["tp"]),
        mesh=mesh,
        in_specs=in_specs,
        out_specs=P("dp", ("kv", "tp"), None),
        check_vma=False,
    )
```

time: 112 us -> 19.3 us (0.17)
  the two profiles are of different devices: /device:TPU:27 before, /device:TPU:0 now
where the time goes in v1:
time: 19.3 us; the launch traced here: 19.1 us
  Pallas kernels  16.8 us (87%)
  local copies, waits for them, and re-layouts  2.3 us (12%)
    pallas_call x1, Pallas kernels, on_device(): pl.pallas_call(functools.partial(kernel, kvn, tpn), out_shape=jax.ShapeDt...  16.8 us
    unnamed x1, local copies, waits for them, and re-layouts  2.3 us

profile of v1, /device:TPU:0, one launch (start us, length us, event | category | flops | bytes accessed | tf_op | source)
XLA Modules:
  0.0 19.1 jit_solution(13052697582778008872)
XLA Ops:
  0.0 16.8 %shard_map.100 = f32[1,128,2048]{2,1,0:T(8,128)} custom-call(bf16[1,256,2048]{2,1,0:T(8,128)(2,1)} %tok_h.1, bf16[2048,384]{1,0:T(8,128)(2,1)} %wq_h.1, bf16[2048,128]{1,0:T(8,128)(2,1)} %wk_h.1, bf16[2048,128]{1,0:T(8,128)(2,1)} %wv_h.1, bf16[24,2048]{1,0:T(8,128)(2,1)} %bitcast.2, f32[2,32,64]{2,1,0:T(8,128)} %cw_h.1, bf16[384,2048]{1,0:T(8,128)(2,1)} %wo_h.1, ...), custom_call_target="tpu_custom_call" | custom-call | tf_op jit(solution)/shard_map/pallas_call | solution.py:442
  16.8 2.3 %copy.12 = f32[1,128,2048]{2,1,0:T(8,128)} copy(f32[1,128,2048]{2,1,0:T(8,128)} %shard_map.100) | data formatting | bytes 2097152

commit v2 on v1

--- a/solution.py
+++ b/solution.py
@@ -74,7 +74,10 @@
     qp,
     qt,
     gt,
-    mixt,
+    part_c,
+    part_n,
+    part_m,
+    part_l,
     mix_own,
     mix_out,
     mix_in,
@@ -195,18 +198,6 @@
     wanted = jnp.sum(pick * ((ja % nb) + 1).astype(F32), axis=1, keepdims=True) - 1.0
     reqs[...] = jnp.broadcast_to(wanted, (kvn * 8, 128)).reshape(kvn, 8, 128)
 
-    pl.semaphore_wait(barrier, kvn)
-    for d in range(1, kvn):
-
-        @pl.when(me >= d)
-        def _():
-            req_copy(d).start()
-
-    weight_copy.start()
-    spread = jnp.where(iota((nb, length), 1) // BLK == iota((nb, length), 0), 1.0, 0.0)
-    member = mm(mm_t(pick, hit), spread)
-    maskb[...] = jnp.where(member > 0.5, 0.0, NEG)
-
     loads[1].wait()
     cos_t = tab[0]
     sin_t = tab[1]
@@ -228,16 +219,57 @@
 
     coarse[0, 0:nb] = compress(key_f, 0)
     coarse[0, nb : 2 * nb] = compress(val_f, 1)
-    for d in range(1, kvn):
-
-        @pl.when(me + d < kvn)
-        def _():
-            coarse_copy(d).start()
-
     half = HEAD // 2
     low = iota((length, cols), 1) % HEAD < half
     swapped = jnp.where(low, pltpu.roll(key_f, cols - half, 1), pltpu.roll(key_f, half, 1))
     tkv[:, 0:cols] = (key_f * cos_n + swapped * sin_n).astype(BF)
+
+    vt[...] = val_f.T.astype(BF)
+
+    pl.semaphore_wait(barrier, kvn)
+    for d in range(1, kvn):
+
+        @pl.when(me >= d)
+        def _():
+            req_copy(d).start()
+
+    for d in range(1, kvn):
+
+        @pl.when(me + d < kvn)
+        def _():
+            coarse_copy(d).start()
+
+    weight_copy.start()
+    spread = jnp.where(iota((nb, length), 1) // BLK == iota((nb, length), 0), 1.0, 0.0)
+    member = mm(mm_t(pick, hit), spread)
+    maskb[...] = jnp.where(member > 0.5, 0.0, NEG)
+
+
+    loads[6].wait()
+    n = rows_out
+    scale = HEAD ** (-0.5)
+    query_t = mm(tok[...], wq[...]).astype(BF).astype(F32).T * scale
+    loads[7].wait()
+    gates = jax.nn.sigmoid(mm_t(wg[...], tok[...]))
+    for h in range(heads):
+        k, g = h // per_kv, h % per_kv
+        first = query_t[h * HEAD : h * HEAD + half]
+        second = query_t[h * HEAD + half : (h + 1) * HEAD]
+        plain = query_t[h * HEAD : (h + 1) * HEAD].astype(BF)
+        turned_low = (first * cos_t - second * sin_t).astype(BF)
+        turned_high = (second * cos_t + first * sin_t).astype(BF)
+        for c in range(tpn):
+            lanes = slice(g * n, (g + 1) * n)
+            here = slice(c * n, (c + 1) * n)
+            qp[c, k, :, lanes] = plain[:, here]
+            qt[c, k, 0:half, lanes] = turned_low[:, here]
+            qt[c, k, half:HEAD, lanes] = turned_high[:, here]
+            for branch in range(2):
+                gate = jnp.zeros((1, n), F32)
+                for t in range(tpn):
+                    row = (branch * tpn + t) * heads + h
+                    gate = jnp.where(tp == t, gates[row : row + 1, here], gate)
+                gt[c, branch * kv_dev + k : branch * kv_dev + k + 1, lanes] = gate
 
     si = iota((slot_rows, length), 0)
     sj = iota((slot_rows, length), 1)
@@ -259,26 +291,6 @@
             blk_out[d - 1, slot_rows : 2 * slot_rows] = sent[:, cols : 2 * cols]
             block_copy(d).start()
 
-    vt[...] = val_f.T.astype(BF)
-
-    loads[6].wait()
-    scale = HEAD ** (-0.5)
-    query_t = mm(tok[...], wq[...]).astype(BF).astype(F32).T * scale
-    qp[...] = query_t.astype(BF)
-    for h in range(heads):
-        first = query_t[h * HEAD : h * HEAD + half]
-        second = query_t[h * HEAD + half : (h + 1) * HEAD]
-        qt[h * HEAD : h * HEAD + half] = (first * cos_t - second * sin_t).astype(BF)
-        qt[h * HEAD + half : (h + 1) * HEAD] = (second * cos_t + first * sin_t).astype(BF)
-    loads[7].wait()
-    gates = jax.nn.sigmoid(mm_t(wg[...], tok[...]))
-    for branch in range(2):
-        mine = jnp.zeros((heads, length), F32)
-        for t in range(tpn):
-            row = (branch * tpn + t) * heads
-            mine = jnp.where(tp == t, gates[row : row + heads], mine)
-        gt[branch * heads : (branch + 1) * heads] = mine
-
     for d in range(1, kvn):
 
         @pl.when(me >= d)
@@ -289,6 +301,29 @@
     coarse_vt = coarse[:, nb : 2 * nb].reshape(kvn * nb, cols).T
     ck = [coarse_k[:, k * HEAD : (k + 1) * HEAD].astype(BF) for k in range(kv_dev)]
     cvt = [coarse_vt[k * HEAD : (k + 1) * HEAD].astype(BF) for k in range(kv_dev)]
+    wide = per_kv * n
+    dk = iota((n, wide), 0)
+    dq = iota((n, wide), 1) % n
+    near_bias = jnp.where((dk // BLK == dq // BLK) & (dk <= dq), 0.0, NEG)
+    cr = iota((kvn * nb, wide), 0)
+    cb = (me - cr // nb) * nb + cr % nb
+    lane = iota((kvn * nb, wide), 1) % n
+    for c in range(tpn):
+        pos = me * length + c * n + lane
+        seen = (cb >= 0) & ((cb + 1) * BLK - 1 <= pos)
+        for k in range(kv_dev):
+            sc = jnp.where(seen, mm(ck[k], qp[c, k]), NEG)
+            near_k = tkv[c * n : (c + 1) * n, k * HEAD : (k + 1) * HEAD]
+            sn = mm(near_k, qt[c, k]) + near_bias
+            peak = jnp.max(sc, axis=0, keepdims=True)
+            top = jnp.max(sn, axis=0, keepdims=True)
+            pw = jnp.where(seen, jnp.exp(sc - peak), 0.0)
+            pn = jnp.exp(sn - top)
+            weight = pw / jnp.maximum(jnp.sum(pw, axis=0, keepdims=True), 1.0)
+            part_c[c, k] = gt[c, k : k + 1] * mm(cvt[k], weight.astype(BF))
+            part_n[c, k] = mm(vt[k * HEAD : (k + 1) * HEAD, c * n : (c + 1) * n], pn.astype(BF))
+            part_m[c, k : k + 1] = top
+            part_l[c, k : k + 1] = jnp.sum(pn, axis=0, keepdims=True)
 
     for d in range(1, kvn):
 
@@ -302,16 +337,8 @@
     kr = [far_k[:, k * HEAD : (k + 1) * HEAD] for k in range(kv_dev)]
     vr = [far_vt[k * HEAD : (k + 1) * HEAD] for k in range(kv_dev)]
 
-    n = rows_out
-    dk = iota((n, n), 0)
-    dq = iota((n, n), 1)
-    near_bias = jnp.where((dk // BLK == dq // BLK) & (dk <= dq), 0.0, NEG)
-    cr = iota((kvn * nb, n), 0)
-    cb = (me - cr // nb) * nb + cr % nb
-
     def attend(chunk):
-        start = pl.multiple_of(chunk * n, n)
-        here = pl.ds(start, n)
+        here = pl.ds(pl.multiple_of(chunk * n, n), n)
         far_bias = jnp.concatenate(
             [
                 jnp.broadcast_to(maskb[d * 8 + s : d * 8 + s + 1, here], (BLK, n))
@@ -320,34 +347,20 @@
             ],
             axis=0,
         )
-        pos = me * length + start + iota((kvn * nb, n), 1)
-        seen = (cb >= 0) & ((cb + 1) * BLK - 1 <= pos)
-        near_k = tkv[here, 0:cols]
-        kd = [near_k[:, k * HEAD : (k + 1) * HEAD] for k in range(kv_dev)]
-        for h in range(heads):
-            k = h // per_kv
-            rows = slice(h * HEAD, (h + 1) * HEAD)
-            sc = jnp.where(seen, mm(ck[k], qp[rows, here]), NEG)
-            peak = jnp.max(sc, axis=0, keepdims=True)
-            pw = jnp.where(seen, jnp.exp(sc - peak), 0.0)
-            weight = pw / jnp.maximum(jnp.sum(pw, axis=0, keepdims=True), 1.0)
-            coarse_out = mm(cvt[k], weight.astype(BF))
-            query = qt[rows, here]
-            sf = mm(kr[k], query) + far_bias
-            sn = mm(kd[k], query) + near_bias
-            top = jnp.maximum(
-                jnp.max(sf, axis=0, keepdims=True), jnp.max(sn, axis=0, keepdims=True)
-            )
+        far_bias = jnp.concatenate([far_bias] * per_kv, axis=1)
+        mixed = []
+        for k in range(kv_dev):
+            sf = mm(kr[k], qt[chunk, k]) + far_bias
+            top_near = part_m[chunk, k : k + 1]
+            top = jnp.maximum(jnp.max(sf, axis=0, keepdims=True), top_near)
+            shrink = jnp.exp(top_near - top)
             pf = jnp.exp(sf - top)
-            pn = jnp.exp(sn - top)
-            norm = jnp.sum(pf, axis=0, keepdims=True) + jnp.sum(pn, axis=0, keepdims=True)
-            fine = mm(vr[k], pf.astype(BF)) + mm(
-                vt[k * HEAD : (k + 1) * HEAD, here], pn.astype(BF)
-            )
-            g_coarse = gt[h : h + 1, here]
-            g_fine = gt[heads + h : heads + h + 1, here]
-            mixt[rows] = g_coarse * coarse_out + fine * (g_fine / norm)
-        return mixt[...].T.astype(BF)
+            norm = jnp.sum(pf, axis=0, keepdims=True) + part_l[chunk, k : k + 1] * shrink
+            fine = mm(vr[k], pf.astype(BF)) + part_n[chunk, k] * shrink
+            g_fine = gt[chunk, kv_dev + k : kv_dev + k + 1]
+            both = part_c[chunk, k] + fine * (g_fine / norm)
+            mixed += [both[:, g * n : (g + 1) * n] for g in range(per_kv)]
+        return jnp.concatenate(mixed, axis=0).T.astype(BF)
 
     mix_out[...] = attend(tpn - 1 - tp)
     mix_copy.start()
@@ -397,6 +410,8 @@
     table = jnp.asarray(rope_table(kvn, length))
     nb = length // BLK
     rows_out = length // tpn
+    kv_dev = cols // HEAD
+    wide = (qcols // cols) * rows_out
     V = pltpu.VMEM
     dma = pltpu.SemaphoreType.DMA
     scratch = [
@@ -418,10 +433,13 @@
         V((kvn, 2 * nb, cols), F32),
         V((kvn - 1, 2 * CAP * BLK, cols), BF),
         V((kvn - 1, 2 * CAP * BLK, cols), BF),
-        V((qcols, length), BF),
-        V((qcols, length), BF),
-        V((wg.shape[1] // tpn, length), F32),
-        V((qcols, rows_out), F32),
+        V((tpn, kv_dev, HEAD, wide), BF),
+        V((tpn, kv_dev, HEAD, wide), BF),
+        V((tpn, 2 * kv_dev, wide), F32),
+        V((tpn, kv_dev, HEAD, wide), F32),
+        V((tpn, kv_dev, HEAD, wide), F32),
+        V((tpn, kv_dev, wide), F32),
+        V((tpn, kv_dev, wide), F32),
         V((rows_out, qcols), BF),
         V((rows_out, qcols), BF),
         V((rows_out, qcols), BF),

time: 19.3 us -> 16.3 us (0.84)
  the two profiles are of different devices: /device:TPU:0 before, /device:TPU:27 now
where the time goes in v2:
time: 16.3 us; the launch traced here: 16.1 us
  Pallas kernels  13.8 us (85%)
  local copies, waits for them, and re-layouts  2.3 us (14%)
    pallas_call x1, Pallas kernels, on_device(): pl.pallas_call(functools.partial(kernel, kvn, tpn), out_shape=jax.ShapeDt...  13.8 us
    unnamed x1, local copies, waits for them, and re-layouts  2.3 us

profile of v2, /device:TPU:27, one launch (start us, length us, event | category | flops | bytes accessed | tf_op | source)
XLA Modules:
  0.0 16.1 jit_solution(17052186145894635033)
XLA Ops:
  0.0 13.8 %shard_map.100 = f32[1,128,2048]{2,1,0:T(8,128)} custom-call(bf16[1,256,2048]{2,1,0:T(8,128)(2,1)} %tok_h.1, bf16[2048,384]{1,0:T(8,128)(2,1)} %wq_h.1, bf16[2048,128]{1,0:T(8,128)(2,1)} %wk_h.1, bf16[2048,128]{1,0:T(8,128)(2,1)} %wv_h.1, bf16[24,2048]{1,0:T(8,128)(2,1)} %bitcast.2, f32[2,32,64]{2,1,0:T(8,128)} %cw_h.1, bf16[384,2048]{1,0:T(8,128)(2,1)} %wo_h.1, ...), custom_call_target="tpu_custom_call" | custom-call | tf_op jit(solution)/shard_map/pallas_call | solution.py:460
  13.8 2.3 %copy.12 = f32[1,128,2048]{2,1,0:T(8,128)} copy(f32[1,128,2048]{2,1,0:T(8,128)} %shard_map.100) | data formatting | bytes 2097152

commit v3 on v2

--- a/solution.py
+++ b/solution.py
@@ -52,7 +52,7 @@
     gain_h,
     chosen_h,
     tab_h,
-    out_h,
+    acc,
     tok,
     wkv,
     wq,
@@ -81,9 +81,7 @@
     mix_own,
     mix_out,
     mix_in,
-    acc,
     lsem,
-    osem,
     req_s,
     req_r,
     co_s,
@@ -198,6 +196,16 @@
     wanted = jnp.sum(pick * ((ja % nb) + 1).astype(F32), axis=1, keepdims=True) - 1.0
     reqs[...] = jnp.broadcast_to(wanted, (kvn * 8, 128)).reshape(kvn, 8, 128)
 
+    @pl.when(me > 0)
+    def _():
+        pl.semaphore_wait(barrier, kvn)
+
+    for d in range(1, kvn):
+
+        @pl.when(me >= d)
+        def _():
+            req_copy(d).start()
+
     loads[1].wait()
     cos_t = tab[0]
     sin_t = tab[1]
@@ -226,12 +234,9 @@
 
     vt[...] = val_f.T.astype(BF)
 
-    pl.semaphore_wait(barrier, kvn)
-    for d in range(1, kvn):
-
-        @pl.when(me >= d)
-        def _():
-            req_copy(d).start()
+    @pl.when(me == 0)
+    def _():
+        pl.semaphore_wait(barrier, kvn)
 
     for d in range(1, kvn):
 
@@ -239,7 +244,6 @@
         def _():
             coarse_copy(d).start()
 
-    weight_copy.start()
     spread = jnp.where(iota((nb, length), 1) // BLK == iota((nb, length), 0), 1.0, 0.0)
     member = mm(mm_t(pick, hit), spread)
     maskb[...] = jnp.where(member > 0.5, 0.0, NEG)
@@ -271,6 +275,20 @@
                     gate = jnp.where(tp == t, gates[row : row + 1, here], gate)
                 gt[c, branch * kv_dev + k : branch * kv_dev + k + 1, lanes] = gate
 
+    wide = per_kv * n
+    dk = iota((n, wide), 0)
+    dq = iota((n, wide), 1) % n
+    near_bias = jnp.where((dk // BLK == dq // BLK) & (dk <= dq), 0.0, NEG)
+    for c in range(tpn):
+        for k in range(kv_dev):
+            near_k = tkv[c * n : (c + 1) * n, k * HEAD : (k + 1) * HEAD]
+            sn = mm(near_k, qt[c, k]) + near_bias
+            top = jnp.max(sn, axis=0, keepdims=True)
+            pn = jnp.exp(sn - top)
+            part_n[c, k] = mm(vt[k * HEAD : (k + 1) * HEAD, c * n : (c + 1) * n], pn.astype(BF))
+            part_m[c, k : k + 1] = top
+            part_l[c, k : k + 1] = jnp.sum(pn, axis=0, keepdims=True)
+
     si = iota((slot_rows, length), 0)
     sj = iota((slot_rows, length), 1)
     for d in range(1, kvn):
@@ -297,14 +315,11 @@
         def _():
             coarse_copy(d).wait_recv()
 
+    weight_copy.start()
     coarse_k = coarse[:, 0:nb].reshape(kvn * nb, cols)
     coarse_vt = coarse[:, nb : 2 * nb].reshape(kvn * nb, cols).T
     ck = [coarse_k[:, k * HEAD : (k + 1) * HEAD].astype(BF) for k in range(kv_dev)]
     cvt = [coarse_vt[k * HEAD : (k + 1) * HEAD].astype(BF) for k in range(kv_dev)]
-    wide = per_kv * n
-    dk = iota((n, wide), 0)
-    dq = iota((n, wide), 1) % n
-    near_bias = jnp.where((dk // BLK == dq // BLK) & (dk <= dq), 0.0, NEG)
     cr = iota((kvn * nb, wide), 0)
     cb = (me - cr // nb) * nb + cr % nb
     lane = iota((kvn * nb, wide), 1) % n
@@ -313,17 +328,10 @@
         seen = (cb >= 0) & ((cb + 1) * BLK - 1 <= pos)
         for k in range(kv_dev):
             sc = jnp.where(seen, mm(ck[k], qp[c, k]), NEG)
-            near_k = tkv[c * n : (c + 1) * n, k * HEAD : (k + 1) * HEAD]
-            sn = mm(near_k, qt[c, k]) + near_bias
             peak = jnp.max(sc, axis=0, keepdims=True)
-            top = jnp.max(sn, axis=0, keepdims=True)
             pw = jnp.where(seen, jnp.exp(sc - peak), 0.0)
-            pn = jnp.exp(sn - top)
             weight = pw / jnp.maximum(jnp.sum(pw, axis=0, keepdims=True), 1.0)
             part_c[c, k] = gt[c, k : k + 1] * mm(cvt[k], weight.astype(BF))
-            part_n[c, k] = mm(vt[k * HEAD : (k + 1) * HEAD, c * n : (c + 1) * n], pn.astype(BF))
-            part_m[c, k : k + 1] = top
-            part_l[c, k : k + 1] = jnp.sum(pn, axis=0, keepdims=True)
 
     for d in range(1, kvn):
 
@@ -368,27 +376,18 @@
     loads[8].wait()
     step = 512
     for c in range(0, width, step):
-        acc[:, c : c + step] = mm(mix_own[...], wo[:, c : c + step])
+        acc[0, :, c : c + step] = mm(mix_own[...], wo[:, c : c + step])
     loads[9].wait()
     weight_copy.wait_recv()
     mix_copy.wait_recv()
     square = jnp.zeros((n, 1), F32)
     for c in range(0, width, step):
-        part = acc[:, c : c + step] + mm(mix_in[...], wo2[:, c : c + step])
-        acc[:, c : c + step] = part
+        part = acc[0, :, c : c + step] + mm(mix_in[...], wo2[:, c : c + step])
+        acc[0, :, c : c + step] = part
         square = square + jnp.sum(part * part, axis=1, keepdims=True)
     factor = lax.rsqrt(square * (1.0 / width) + EPS)
-    pieces = 4
-    span = n // pieces
-    stores = []
-    for i in range(pieces):
-        rows = slice(i * span, (i + 1) * span)
-        acc[rows] = acc[rows] * factor[rows] * gain[...]
-        store = pltpu.make_async_copy(acc.at[pl.ds(i * span, span)], out_h.at[0, pl.ds(i * span, span)], osem.at[i])
-        store.start()
-        stores.append(store)
-    for store in stores:
-        store.wait()
+    for c in range(0, width, step):
+        acc[0, :, c : c + step] = acc[0, :, c : c + step] * factor * gain[:, c : c + step]
     weight_copy.wait_send()
     mix_copy.wait_send()
     for d in range(1, kvn):
@@ -443,9 +442,7 @@
         V((rows_out, qcols), BF),
         V((rows_out, qcols), BF),
         V((rows_out, qcols), BF),
-        V((rows_out, width), F32),
         dma((10,)),
-        dma((4,)),
         dma((kvn,)),
         dma((kvn,)),
         dma((kvn,)),
@@ -459,12 +456,12 @@
     ]
     return pl.pallas_call(
         functools.partial(kernel, kvn, tpn),
-        out_shape=jax.ShapeDtypeStruct((1, rows_out, width), F32),
+        out_shape=pltpu.VMEM((1, rows_out, width), F32),
         in_specs=[ANY] * 10,
-        out_specs=ANY,
+        out_specs=pl.BlockSpec(memory_space=pltpu.VMEM),
         scratch_shapes=scratch,
         compiler_params=pltpu.CompilerParams(
-            collective_id=0, has_side_effects=True, vmem_limit_bytes=67043328
+            collective_id=0, has_side_effects=True, vmem_limit_bytes=60000000
         ),
     )(tokens, wq, wk, wv, wg.T, cw, wo, gain.reshape(1, width), chosen, table)
 

time: 16.3 us -> 13.8 us (0.85)
  local copies, waits for them, and re-layouts: 2.3 us -> 0.97 us
  Pallas kernels: 13.8 us -> 12.7 us
    unnamed x1, local copies, waits for them, and re-layouts: 2.3 us -> 0.97 us
    pallas_call x1, Pallas kernels: 13.8 us -> 12.7 us  [on_device(): pl.pallas_call(functools.partial(kernel, kvn, tpn), out_shape=pltpu.VMEM(...]
where the time goes in v3:
time: 13.8 us; the launch traced here: 13.6 us
  Pallas kernels  12.7 us (92%)
  local copies, waits for them, and re-layouts  0.97 us (7%)
    pallas_call x1, Pallas kernels, on_device(): pl.pallas_call(functools.partial(kernel, kvn, tpn), out_shape=pltpu.VMEM(...  12.7 us
    unnamed x1, local copies, waits for them, and re-layouts  0.97 us

profile of v3, /device:TPU:27, one launch (start us, length us, event | category | flops | bytes accessed | tf_op | source)
XLA Modules:
  0.0 13.6 jit_solution(1076501727337368809)
XLA Ops:
  0.0 12.7 %shard_map.100 = f32[1,128,2048]{2,1,0:T(8,128)S(1)} custom-call(bf16[1,256,2048]{2,1,0:T(8,128)(2,1)} %tok_h.1, bf16[2048,384]{1,0:T(8,128)(2,1)} %wq_h.1, bf16[2048,128]{1,0:T(8,128)(2,1)} %wk_h.1, bf16[2048,128]{1,0:T(8,128)(2,1)} %wv_h.1, bf16[24,2048]{1,0:T(8,128)(2,1)} %bitcast.2, f32[2,32,64]{2,1,0:T(8,128)} %cw_h.1, bf16[384,2048]{1,0:T(8,128)(2,1)} %wo_h.1, ...), custom_call_target="tpu_custom_call" | custom-call | tf_op jit(solution)/shard_map/pallas_call | solution.py:457
  12.7 1.0 %copy.12 = f32[1,128,2048]{2,1,0:T(8,128)} copy(f32[1,128,2048]{2,1,0:T(8,128)S(1)} %shard_map.100) | data formatting | bytes 2097152

commit v4 on v3

--- a/solution.py
+++ b/solution.py
@@ -172,6 +172,15 @@
             blks[d - 1] = jnp.zeros(blks.shape[1:], BF)
             coarse[d] = jnp.zeros(coarse.shape[1:], F32)
 
+    def publish():
+        for d in range(1, kvn):
+
+            @pl.when(me + d < kvn)
+            def _():
+                coarse_copy(d).start()
+
+        weight_copy.start()
+
     loads[0].wait()
     listed = chosen[...]
     lane_blk = iota((nb, total_blocks), 1)
@@ -234,15 +243,9 @@
 
     vt[...] = val_f.T.astype(BF)
 
-    @pl.when(me == 0)
+    @pl.when(me > 0)
     def _():
-        pl.semaphore_wait(barrier, kvn)
-
-    for d in range(1, kvn):
-
-        @pl.when(me + d < kvn)
-        def _():
-            coarse_copy(d).start()
+        publish()
 
     spread = jnp.where(iota((nb, length), 1) // BLK == iota((nb, length), 0), 1.0, 0.0)
     member = mm(mm_t(pick, hit), spread)
@@ -253,8 +256,6 @@
     n = rows_out
     scale = HEAD ** (-0.5)
     query_t = mm(tok[...], wq[...]).astype(BF).astype(F32).T * scale
-    loads[7].wait()
-    gates = jax.nn.sigmoid(mm_t(wg[...], tok[...]))
     for h in range(heads):
         k, g = h // per_kv, h % per_kv
         first = query_t[h * HEAD : h * HEAD + half]
@@ -268,6 +269,43 @@
             qp[c, k, :, lanes] = plain[:, here]
             qt[c, k, 0:half, lanes] = turned_low[:, here]
             qt[c, k, half:HEAD, lanes] = turned_high[:, here]
+
+    @pl.when(me == 0)
+    def _():
+        pl.semaphore_wait(barrier, kvn)
+        publish()
+
+    si = iota((slot_rows, length), 0)
+    sj = iota((slot_rows, length), 1)
+
+    def serve(d):
+        req_copy(d).wait_recv()
+        tile = reqin[d]
+        ask = jnp.concatenate(
+            [jnp.broadcast_to(tile[s : s + 1], (BLK, 128)) for s in range(CAP)], axis=0
+        )
+        ask = jnp.concatenate([ask] * (length // 128), axis=1)
+        chooser = jnp.where(
+            (ask == (sj // BLK).astype(F32)) & (si % BLK == sj % BLK), 1.0, 0.0
+        ).astype(BF)
+        sent = mm(chooser, tkv[...]).astype(BF)
+        blk_out[d - 1, 0:slot_rows] = sent[:, 0:cols]
+        blk_out[d - 1, slot_rows : 2 * slot_rows] = sent[:, cols : 2 * cols]
+        block_copy(d).start()
+
+    for d in reversed(range(1, kvn)):
+
+        @pl.when((me > 0) & (me + d < kvn))
+        def _():
+            serve(d)
+
+    loads[7].wait()
+    gates = jax.nn.sigmoid(mm_t(wg[...], tok[...]))
+    for h in range(heads):
+        k, g = h // per_kv, h % per_kv
+        for c in range(tpn):
+            lanes = slice(g * n, (g + 1) * n)
+            here = slice(c * n, (c + 1) * n)
             for branch in range(2):
                 gate = jnp.zeros((1, n), F32)
                 for t in range(tpn):
@@ -289,33 +327,18 @@
             part_m[c, k : k + 1] = top
             part_l[c, k : k + 1] = jnp.sum(pn, axis=0, keepdims=True)
 
-    si = iota((slot_rows, length), 0)
-    sj = iota((slot_rows, length), 1)
+    for d in range(1, kvn - 1):
+
+        @pl.when((me == 0) & (me + d < kvn))
+        def _():
+            serve(d)
+
     for d in range(1, kvn):
 
-        @pl.when(me + d < kvn)
-        def _():
-            req_copy(d).wait_recv()
-            tile = reqin[d]
-            ask = jnp.concatenate(
-                [jnp.broadcast_to(tile[s : s + 1], (BLK, 128)) for s in range(CAP)], axis=0
-            )
-            ask = jnp.concatenate([ask] * (length // 128), axis=1)
-            chooser = jnp.where(
-                (ask == (sj // BLK).astype(F32)) & (si % BLK == sj % BLK), 1.0, 0.0
-            ).astype(BF)
-            sent = mm(chooser, tkv[...]).astype(BF)
-            blk_out[d - 1, 0:slot_rows] = sent[:, 0:cols]
-            blk_out[d - 1, slot_rows : 2 * slot_rows] = sent[:, cols : 2 * cols]
-            block_copy(d).start()
-
-    for d in range(1, kvn):
-
         @pl.when(me >= d)
         def _():
             coarse_copy(d).wait_recv()
 
-    weight_copy.start()
     coarse_k = coarse[:, 0:nb].reshape(kvn * nb, cols)
     coarse_vt = coarse[:, nb : 2 * nb].reshape(kvn * nb, cols).T
     ck = [coarse_k[:, k * HEAD : (k + 1) * HEAD].astype(BF) for k in range(kv_dev)]
@@ -332,6 +355,10 @@
             pw = jnp.where(seen, jnp.exp(sc - peak), 0.0)
             weight = pw / jnp.maximum(jnp.sum(pw, axis=0, keepdims=True), 1.0)
             part_c[c, k] = gt[c, k : k + 1] * mm(cvt[k], weight.astype(BF))
+
+    @pl.when((me == 0) & (kvn > 1))
+    def _():
+        serve(kvn - 1)
 
     for d in range(1, kvn):
 

time: 13.8 us -> 13.5 us (0.978)
  Pallas kernels: 12.7 us -> 12.3 us
    pallas_call x1, Pallas kernels: 12.7 us -> 12.3 us  [on_device(): pl.pallas_call(functools.partial(kernel, kvn, tpn), out_shape=pltpu.VMEM(...]
where the time goes in v4:
time: 13.5 us; the launch traced here: 13.3 us
  Pallas kernels  12.3 us (91%)
  local copies, waits for them, and re-layouts  0.97 us (7%)
    pallas_call x1, Pallas kernels, on_device(): pl.pallas_call(functools.partial(kernel, kvn, tpn), out_shape=pltpu.VMEM(...  12.3 us
    unnamed x1, local copies, waits for them, and re-layouts  0.97 us

profile of v4, /device:TPU:27, one launch (start us, length us, event | category | flops | bytes accessed | tf_op | source)
XLA Modules:
  0.0 13.3 jit_solution(18360203165013554930)
XLA Ops:
  0.0 12.3 %shard_map.100 = f32[1,128,2048]{2,1,0:T(8,128)S(1)} custom-call(bf16[1,256,2048]{2,1,0:T(8,128)(2,1)} %tok_h.1, bf16[2048,384]{1,0:T(8,128)(2,1)} %wq_h.1, bf16[2048,128]{1,0:T(8,128)(2,1)} %wk_h.1, bf16[2048,128]{1,0:T(8,128)(2,1)} %wv_h.1, bf16[24,2048]{1,0:T(8,128)(2,1)} %bitcast.2, f32[2,32,64]{2,1,0:T(8,128)} %cw_h.1, bf16[384,2048]{1,0:T(8,128)(2,1)} %wo_h.1, ...), custom_call_target="tpu_custom_call" | custom-call | tf_op jit(solution)/shard_map/pallas_call | solution.py:484
  12.3 1.0 %copy.12 = f32[1,128,2048]{2,1,0:T(8,128)} copy(f32[1,128,2048]{2,1,0:T(8,128)S(1)} %shard_map.100) | data formatting | bytes 2097152
